TPU v7x, 32 devices: a whole 2x2x4 slice. The times are simulated.
32 devices in a mesh: grp: 2 (over y), ep: 8 (over z, x), tp: 2 (over core).
Axes of the slice: x: 2, y: 2, z: 4, core: 2. Of those that a mesh axis runs over, the one named last changes fastest.
Arguments:
- tokens: bfloat16 [1024, 2048], P(('grp', 'ep')), parts along dimension 0, may hold values from -6 to 6
- chosen: int32 [1, 16, 9], P(None, ('grp', 'ep')), parts along dimension 1, may hold values from -1 to 63, as said below
- route_weight: float32 [1, 16, 9], P(None, ('grp', 'ep')), parts along dimension 1, may hold values from 0.1 to 1
- expert_gate: bfloat16 [2048, 4096], P(None, ('ep', 'tp')), may hold values from -0.125 to 0.125
- expert_up: bfloat16 [2048, 4096], P(None, ('ep', 'tp')), may hold values from -0.125 to 0.125
- expert_down: bfloat16 [4096, 2048], P(('ep', 'tp')), may hold values from -0.09375 to 0.09375
- dense_gate: bfloat16 [2048, 512], P('ep', 'tp'), may hold values from -0.125 to 0.125
- dense_up: bfloat16 [2048, 512], P('ep', 'tp'), may hold values from -0.125 to 0.125
- dense_down: bfloat16 [512, 2048], P('tp', 'ep'), may hold values from -0.25 to 0.25
- branch_gate: float32 [2048], P('tp'), may hold values from -6 to 6
Outputs:
- mixed: bfloat16 [1024, 2048], P(('grp', 'ep'), 'tp'), parts along dimension 0
There are 2 independent parts, one for each index of `grp`. A program takes and returns all parts, laid end to end along the dimension named above; an argument that names none is the same for every part. Nothing has to cross between parts.
Inputs may be any that keep to these rules, and one draw needn't show every extreme that they name: chosen[e, s, k] is -1 or an index local to device s (token s * 64 + chosen[e, s, k] of the whole). In each (e, s) row the live entries come first and are distinct, the -1 entries follow. Each expert takes exactly 64 tokens in all, at most 9 from one device, and for every expert some device gives it exactly 9.
All inputs are finite; a program needn't handle non-finite values.
Results may differ from a plain program's by a relative error of at most 0.0085.
Values may be sent and summed in bfloat16 or wider, within the bound.
A program may use at most 64 MiB of HBM per device.

v0:
```python
import jax
import jax.numpy as jnp
from jax import lax
from jax.sharding import PartitionSpec as P


def swapped(block, axis, apart):
    count = lax.axis_size(axis)
    route = []
    for low in range(count):
        high = low | 1 << apart
        if high != low and high < count:
            route += [(low, high), (high, low)]
    return lax.ppermute(block, axis, route)


def expert_hidden(received, gate_cols, up_cols):
    flat_rows = received.reshape(-1, received.shape[-1])
    gate_act = jnp.dot(flat_rows, gate_cols, preferred_element_type=jnp.float32)
    up_act = jnp.dot(flat_rows, up_cols, preferred_element_type=jnp.float32)
    hidden = (jax.nn.silu(gate_act) * up_act).astype(jnp.bfloat16)
    return hidden.reshape(received.shape[0], received.shape[1], gate_cols.shape[1])


def join_pieces(mine, theirs, upper):
    return jnp.where(upper, jnp.concatenate([theirs, mine], 2), jnp.concatenate([mine, theirs], 2))


def local(
    tokens,
    chosen,
    route_weight,
    expert_gate,
    expert_up,
    expert_down,
    dense_gate,
    dense_up,
    dense_down,
    branch_gate,
):
    ep_count = lax.axis_size("ep")
    experts = chosen.shape[0]
    slots = chosen.shape[2]
    tok_local = tokens.shape[0]
    width = tokens.shape[1]
    picked = chosen[:, 0, :]
    filled = picked >= 0
    token_rows = jnp.take(tokens, jnp.maximum(picked, 0).reshape(-1), axis=0).reshape(
        experts, slots, width
    )
    token_rows = jnp.where(filled[:, :, None], token_rows, jnp.zeros((), jnp.bfloat16))
    send_width = token_rows.shape[2]
    piece = send_width // 8
    split_rows = jnp.transpose(token_rows.reshape(experts, slots, 8, piece), (0, 2, 1, 3)).reshape(
        ep_count, slots, piece
    )
    own_piece = lax.all_to_all(split_rows, "ep", split_axis=0, concat_axis=0, tiled=True)
    member = lax.axis_index("ep") % 8
    current = own_piece[:, :, None, :]
    partner = swapped(current, "ep", 0)
    current = join_pieces(current, partner, member % 2 == 1)
    partner = swapped(current, "ep", 1)
    current = join_pieces(current, partner, member // 2 % 2 == 1)
    partner = swapped(current, "ep", 2)
    current = join_pieces(current, partner, member // 4 == 1)
    received = current.reshape(ep_count, slots, send_width)
    hidden = expert_hidden(received, gate_cols=expert_gate, up_cols=expert_up)
    flat_hidden = hidden.reshape(ep_count * slots, -1)
    shard_rows = expert_down
    member_sums = lax.psum_scatter(
        lax.dot_general(
            shard_rows, flat_hidden, (((0,), (1,)), ((), ())), preferred_element_type=jnp.float32
        ).astype(jnp.bfloat16),
        "tp",
        scatter_dimension=0,
        tiled=True,
    )
    returned = lax.all_to_all(member_sums, "ep", split_axis=1, concat_axis=1, tiled=True)
    summed = returned.astype(jnp.float32).reshape(width // 2, experts, 8, slots).sum(axis=2)
    positions = lax.broadcasted_iota(jnp.int32, (experts, slots, tok_local), 2)
    weights_table = jnp.where(picked[:, :, None] == positions, route_weight[:, 0, :, None], 0.0)
    combined = jnp.einsum("fek,ekt->tf", summed, weights_table, precision=lax.Precision.HIGHEST)
    shard_rows = (
        lax.all_gather(dense_gate, "ep", axis=0, tiled=True),
        lax.all_gather(dense_up, "ep", axis=0, tiled=True),
    )
    gate_dense = jnp.dot(tokens, shard_rows[0], preferred_element_type=jnp.float32)
    up_dense = jnp.dot(tokens, shard_rows[1], preferred_element_type=jnp.float32)
    dense_hidden = (jax.nn.silu(gate_dense) * up_dense).astype(jnp.bfloat16)
    dense_terms = jnp.dot(
        dense_hidden,
        lax.all_gather(dense_down, "ep", axis=1, tiled=True),
        preferred_element_type=jnp.float32,
    )
    dense_sum = lax.psum_scatter(
        dense_terms.astype(jnp.bfloat16), "tp", scatter_dimension=1, tiled=True
    ).astype(jnp.float32)
    return (combined + jax.nn.sigmoid(branch_gate)[None, :] * dense_sum).astype(jnp.bfloat16)


def solution(mesh):
    return jax.shard_map(
        local,
        mesh=mesh,
        in_specs=(
            P(("grp", "ep"), None),
            P(None, ("grp", "ep"), None),
            P(None, ("grp", "ep"), None),
            P(None, ("ep", "tp")),
            P(None, ("ep", "tp")),
            P(("ep", "tp"), None),
            P("ep", "tp"),
            P("ep", "tp"),
            P("tp", "ep"),
            P("tp"),
        ),
        out_specs=P(("grp", "ep"), "tp"),
        check_vma=False,
    )
```

profile of v0, /device:TPU:0, one launch (start us, length us, event | category | flops | bytes accessed | tf_op | source)
XLA Modules:
  0.0 162.1 jit_solution(17605187083843992932)
XLA Ops:
  7.4 0.0 copy-start
  7.4 0.0 copy-start.1
  7.4 0.0 all-gather.4.cloned.1.call-start
  7.4 0.7 all-gather.4.cloned.1.call-update
  8.1 0.0 all-gather.6.cloned.1.call-start
  8.1 0.7 all-gather.6.cloned.1.call-update
  8.8 0.0 copy-start.4
  8.9 0.0 all-gather.8.cloned.1.call-start
  8.9 0.7 all-gather.8.cloned.1.call-update
  9.6 0.0 reduce-scatter.3.cloned.1.call-start
  9.6 0.0 copy-done.4
  9.7 0.0 copy-done.1
  9.7 0.6 gather_fusion
  10.3 0.1 fusion.10
  10.4 14.1 %all_to_all.14 = bf16[8,9,256]{2,1,0:T(8,128)(2,1)S(1)} all-to-all(bf16[8,9,256]{2,1,0:T(8,128)(2,1)S(1)} %fusion.10), channel_id=1, replica_groups=mesh['grp'=2,'ep'=8,'tp'=2] {'ep'}, dimensions={0} | all-to-all | bytes 73728 | tf_op jit(solution)/shard_map/all_to_all | solution.py:57
  24.5 0.4 collective-permute-start
  24.9 3.7 %collective-permute-done = bf16[8,9,1,256]{3,0,2,1:T(8,128)(2,1)S(1)} collective-permute-done((bf16[8,9,1,256]{3,0,2,1:T(8,128)(2,1)S(1)}, bf16[8,9,1,256]{3,0,2,1:T(8,128)(2,1)S(1)}, u32[]{:S(2)}, u32[]{:S(2)}) %collective-permute-start) | collective-permute-done | bytes 36896 | tf_op jit(solution)/shard_map/ppermute | solution.py:14
  28.5 0.2 collective-permute-start.1
  28.7 0.0 copy-start.2
  28.7 4.7 %collective-permute-done.1 = bf16[8,9,2,256]{3,0,2,1:T(8,128)(2,1)S(1)} collective-permute-done((bf16[8,9,2,256]{3,0,2,1:T(8,128)(2,1)S(1)}, bf16[8,9,2,256]{3,0,2,1:T(8,128)(2,1)S(1)}, u32[]{:S(2)}, u32[]{:S(2)}) %collective-permute-start.1) | collective-permute-done | bytes 73760 | tf_op jit(solution)/shard_map/ppermute | solution.py:14
  33.5 0.5 collective-permute-start.2
  34.0 6.7 %collective-permute-done.2 = bf16[8,9,4,256]{3,0,2,1:T(8,128)(2,1)S(1)} collective-permute-done((bf16[8,9,4,256]{3,0,2,1:T(8,128)(2,1)S(1)}, bf16[8,9,4,256]{3,0,2,1:T(8,128)(2,1)S(1)}, u32[]{:S(2)}, u32[]{:S(2)}) %collective-permute-start.2) | collective-permute-done | bytes 147488 | tf_op jit(solution)/shard_map/ppermute | solution.py:14
  40.7 0.1 copy.15
  40.8 0.1 copy.17
  40.9 0.0 copy-done.2
  40.9 0.3 fusion.25
  41.2 0.0 copy-done
  41.2 2.7 %fusion = bf16[2048,72]{0,1:T(8,128)(2,1)} fusion(bf16[256,2048]{1,0:T(8,128)(2,1)S(1)} %copy-done, bf16[72,2048]{1,0:T(8,128)(2,1)S(1)} %bitcast.37, bf16[2048,256]{1,0:T(8,128)(2,1)} %param.14, f32[72,256]{1,0:T(8,128)S(1)} %fusion.25), kind=kOutput, calls=%fused_computation.3 | convolution fusion | flops 151252992 | bytes 2760704 | tf_op jit(solution)/shard_map/dot_general | solution.py:71
  43.9 0.0 reduce-scatter.3.cloned.1.call-update
  43.9 0.0 reduce-scatter.5.cloned.1.call-start
  44.0 10.2 %all-gather.4.cloned.1.call-done = bf16[2048,256]{1,0:T(8,128)(2,1)} async-done(((bf16[256,256]{1,0:T(8,128)(2,1)}), bf16[2048,256]{1,0:T(8,128)(2,1)}) %all-gather.4.cloned.1.call-update) | async-done | bytes 1048592 | tf_op jit(solution)/shard_map/all_gather | solution.py:84
  54.2 1.5 fusion.26
  55.7 39.6 %all-gather.6.cloned.1.call-done = bf16[2048,256]{1,0:T(8,128)(2,1)} async-done(((bf16[256,256]{1,0:T(8,128)(2,1)}), bf16[2048,256]{1,0:T(8,128)(2,1)}) %all-gather.6.cloned.1.call-update) | async-done | bytes 1048592 | tf_op jit(solution)/shard_map/all_gather | solution.py:85
  95.3 40.2 %all-gather.8.cloned.1.call-done = bf16[256,2048]{1,0:T(8,128)(2,1)} async-done(((bf16[256,256]{1,0:T(8,128)(2,1)}), bf16[256,2048]{1,0:T(8,128)(2,1)}) %all-gather.8.cloned.1.call-update) | async-done | bytes 1048592 | tf_op jit(solution)/shard_map/all_gather | solution.py:92
  135.4 3.1 %convolution_convert_fusion.1 = bf16[64,2048]{1,0:T(8,128)(2,1)} fusion(bf16[256,2048]{1,0:T(8,128)(2,1)} %all-gather.8.cloned.1.call-done, bf16[64,2048]{1,0:T(8,128)(2,1)S(1)} %copy-done.1, bf16[2048,256]{1,0:T(8,128)(2,1)} %all-gather.6.cloned.1.call-done, f32[64,256]{1,0:T(8,128)S(1)} %fusion.26), kind=kOutput, calls=%fused_computation.2 | convolution fusion | flops 134447104 | bytes 2686976 | tf_op jit(solution)/shard_map/dot_general | solution.py:90
  138.5 0.0 reduce-scatter.5.cloned.1.call-update
  138.5 0.0 reduce-scatter.3.cloned.1.call-done
  138.6 1.7 %all_to_all.10 = bf16[1024,8,9]{0,2,1:T(8,128)(2,1)} reshape(bf16[1024,72]{0,1:T(8,128)(2,1)} %reduce-scatter.3.cloned.1.call-done) | data formatting | bytes 294912 | tf_op jit(solution)/shard_map/all_to_all | solution.py:78
  140.2 0.0 copy-start.3
  140.2 3.8 %all-to-all-start.1 = ((bf16[1024,8,9]{0,2,1:T(8,128)(2,1)}), bf16[1024,8,9]{0,2,1:T(8,128)(2,1)S(1)}, u32[]{:S(2)}, u32[]{:S(2)}) async-start(bf16[1024,8,9]{0,2,1:T(8,128)(2,1)} %all_to_all.10), calls=%async_computation.2 | async-start | bytes 524288 | tf_op jit(solution)/shard_map/all_to_all | solution.py:78
  144.0 0.0 copy-done.3
  144.0 8.2 %all-to-all-done.1 = bf16[1024,8,9]{0,2,1:T(8,128)(2,1)S(1)} async-done(((bf16[1024,8,9]{0,2,1:T(8,128)(2,1)}), bf16[1024,8,9]{0,2,1:T(8,128)(2,1)S(1)}, u32[]{:S(2)}, u32[]{:S(2)}) %all-to-all-start.1) | async-done | bytes 147488 | tf_op jit(solution)/shard_map/all_to_all | solution.py:78
  152.3 0.0 reduce-scatter.5.cloned.1.call-done
  152.3 0.0 copy-start.5
  152.3 0.6 copy-done.5
  153.0 2.0 %fusion.1 = bf16[64,1024]{1,0:T(8,128)(2,1)} fusion(f32[1024,9]{0,1:T(8,128)S(1)} %convert_reduce_fusion, bf16[64,1024]{1,0:T(8,128)(2,1)} %reduce-scatter.5.cloned.1.call-done, f32[1024]{0:T(1024)S(1)} %add_divide_fusion, f32[9]{0:T(128)S(1)} %bitcast.44, s32[9]{0:T(128)S(1)} %bitcast.43), kind=kOutput, calls=%fused_computation.5 | convolution fusion | flops 7341184 | bytes 303176 | tf_op jit(solution)/shard_map/fek,ekt->tf/dot_general | solution.py:82
  (11 shorter events, 0.2 us)
Async XLA Ops:
  7.4 33.8 %copy-start = (bf16[256,2048]{1,0:T(8,128)(2,1)S(1)}, bf16[256,2048]{1,0:T(8,128)(2,1)}, u32[]{:S(2)}) copy-start(bf16[256,2048]{1,0:T(8,128)(2,1)} %param.15) | copy-start | bytes 3145732
  7.4 2.3 %copy-start.1 = (bf16[64,2048]{1,0:T(8,128)(2,1)S(1)}, bf16[64,2048]{1,0:T(8,128)(2,1)}, u32[]{:S(2)}) copy-start(bf16[64,2048]{1,0:T(8,128)(2,1)} %param.10) | copy-start | bytes 786436
  7.4 46.8 %all-gather.4.cloned.1.call-start = ((), (), s32[]{:S(2)}) async-start(), calls=%async_computation.5 | async-start | bytes 1179648 | tf_op jit(solution)/shard_map/all_gather | solution.py:84
  8.1 87.2 %all-gather.6.cloned.1.call-start = ((), (), s32[]{:S(2)}) async-start(), calls=%async_computation.6 | async-start | bytes 1179648 | tf_op jit(solution)/shard_map/all_gather | solution.py:85
  8.8 0.8 copy-start.4
  8.9 126.6 %all-gather.8.cloned.1.call-start = ((), (), s32[]{:S(2)}) async-start(), calls=%async_computation.7 | async-start | bytes 1179648 | tf_op jit(solution)/shard_map/all_gather | solution.py:92
  9.6 129.0 %reduce-scatter.3.cloned.1.call-start = ((), (), s32[]{:S(2)}) async-start(), calls=%async_computation.4 | async-start | bytes 442368 | tf_op jit(solution)/shard_map/reduce_scatter | solution.py:70
  24.5 4.0 %collective-permute-start = (bf16[8,9,1,256]{3,0,2,1:T(8,128)(2,1)S(1)}, bf16[8,9,1,256]{3,0,2,1:T(8,128)(2,1)S(1)}, u32[]{:S(2)}, u32[]{:S(2)}) collective-permute-start(bf16[8,9,1,256]{3,0,2,1:T(8,128)(2,1)S(1)} %bitcast.41), channel_id=1, source_target_pairs={{0,2},{2,0},{4,6},{6,4},{8,10},{10,8},{12,14},{14,12},{1,3},{3,1},... | collective-permute-start | bytes 110600 | tf_op jit(solution)/shard_map/ppermute | solution.py:14
  28.5 4.9 %collective-permute-start.1 = (bf16[8,9,2,256]{3,0,2,1:T(8,128)(2,1)S(1)}, bf16[8,9,2,256]{3,0,2,1:T(8,128)(2,1)S(1)}, u32[]{:S(2)}, u32[]{:S(2)}) collective-permute-start(bf16[8,9,2,256]{3,0,2,1:T(8,128)(2,1)S(1)} %maximum_select_fusion.2), channel_id=1, source_target_pairs={{0,4},{4,0},{2,6},{6,2},{8,12},{12,8},{10,14},{14,10},{1,5},{5,1},... | collective-permute-start | bytes 221192 | tf_op jit(solution)/shard_map/ppermute | solution.py:14
  28.7 12.1 %copy-start.2 = (bf16[2048,256]{1,0:T(8,128)(2,1)S(1)}, bf16[2048,256]{1,0:T(8,128)(2,1)}, u32[]{:S(2)}) copy-start(bf16[2048,256]{1,0:T(8,128)(2,1)} %param.13) | copy-start | bytes 3145732
  33.5 7.2 %collective-permute-start.2 = (bf16[8,9,4,256]{3,0,2,1:T(8,128)(2,1)S(1)}, bf16[8,9,4,256]{3,0,2,1:T(8,128)(2,1)S(1)}, u32[]{:S(2)}, u32[]{:S(2)}) collective-permute-start(bf16[8,9,4,256]{3,0,2,1:T(8,128)(2,1)S(1)} %maximum_select_fusion.1), channel_id=1, source_target_pairs={{0,8},{8,0},{2,10},{10,2},{4,12},{12,4},{6,14},{14,6},{1,9},{9,1},... | collective-permute-start | bytes 442376 | tf_op jit(solution)/shard_map/ppermute | solution.py:14
  43.9 108.4 %reduce-scatter.5.cloned.1.call-start = ((), (), s32[]{:S(2)}) async-start(), calls=%async_computation.8 | async-start | bytes 393216 | tf_op jit(solution)/shard_map/reduce_scatter | solution.py:95
  140.2 3.8 %copy-start.3 = (f32[1024]{0:T(1024)S(1)}, f32[1024]{0:T(1024)}, u32[]{:S(2)}) copy-start(f32[1024]{0:T(1024)} %param.19) | copy-start | bytes 12292
  140.2 12.0 %all-to-all-start.1 = ((bf16[1024,8,9]{0,2,1:T(8,128)(2,1)}), bf16[1024,8,9]{0,2,1:T(8,128)(2,1)S(1)}, u32[]{:S(2)}, u32[]{:S(2)}) async-start(bf16[1024,8,9]{0,2,1:T(8,128)(2,1)} %all_to_all.10), calls=%async_computation.2 | async-start | bytes 524288 | tf_op jit(solution)/shard_map/all_to_all | solution.py:78
  152.3 0.7 copy-start.5
Sparse Core Ops, SparseCore 0:
  10.3 43.8 all-gather.3
  56.3 38.9 all-gather.5
  97.3 38.0 all-gather.7
Sparse Core Ops, SparseCore 1:
  44.0 5.7 reduce-scatter.2
  138.6 6.7 reduce-scatter.4
where the time goes:
time: 163 us; the launch traced here: 162 us
  waiting for transfers between devices  115 us (71%)
  between operations  14.7 us (9%)
  blocking collectives  14.1 us (9%)
  matrix products  9.66 us (6%)
  starting transfers between devices  4.97 us (3%)
  local copies, waits for them, and re-layouts  3.09 us (2%)
    all_gather x1, waiting for transfers between devices, local(): lax.all_gather(dense_down, 'ep', axis=1, tiled=True)  40.2 us
    all_gather x1, waiting for transfers between devices, local(): lax.all_gather(dense_up, 'ep', axis=0, tiled=True)  39.6 us
    ppermute x3, waiting for transfers between devices, swapped(): return lax.ppermute(block, axis, route)  15.1 us
    all_to_all x1, blocking collectives, local(): lax.all_to_all(split_rows, 'ep', split_axis=0, concat_axis=0, tiled=True)  14.1 us
    all_gather x1, waiting for transfers between devices, local(): lax.all_gather(dense_gate, 'ep', axis=0, tiled=True)  10.2 us
    all_to_all x1, waiting for transfers between devices, local(): lax.all_to_all(member_sums, 'ep', split_axis=1, concat_axis=1, tiled=True)  8.21 us
    all_to_all x1, starting transfers between devices, local(): lax.all_to_all(member_sums, 'ep', split_axis=1, concat_axis=1, tiled=True)  3.76 us
  transfers between devices with their start and end apart: 9, of which 7 were waited for; matrix products, arithmetic and copies ran while one was open for 5% of the time, Pallas kernels for 0%

commit v1 on v0

--- a/solution.py
+++ b/solution.py
@@ -75,7 +75,10 @@
         scatter_dimension=0,
         tiled=True,
     )
-    returned = lax.all_to_all(member_sums, "ep", split_axis=1, concat_axis=1, tiled=True)
+    returned = jnp.concatenate(
+        lax.all_to_all(jnp.stack(jnp.split(member_sums, lax.axis_size("ep"), axis=1)), "ep", 0, 0),
+        axis=1,
+    )
     summed = returned.astype(jnp.float32).reshape(width // 2, experts, 8, slots).sum(axis=2)
     positions = lax.broadcasted_iota(jnp.int32, (experts, slots, tok_local), 2)
     weights_table = jnp.where(picked[:, :, None] == positions, route_weight[:, 0, :, None], 0.0)

time: 163 us -> 193 us (1.18)
  waiting for transfers between devices: 115 us -> 134 us
  local copies, waits for them, and re-layouts: 3.09 us -> 15.2 us
    all_gather x1, waiting for transfers between devices: 10.2 us -> 25.1 us  [local(): lax.all_gather(dense_gate, 'ep', axis=0, tiled=True)]
    unnamed x14 -> x23, local copies, waits for them, and re-layouts: 0.74 us -> 12.1 us
    reduce_scatter x1, waiting for transfers between devices: 0.03 us -> 4.29 us  [local(): lax.psum_scatter(lax.dot_general(shard_rows, flat_hidden, (((0,), (1,)),...]
  transfers between devices with their start and end apart: 9 -> 9, of which waited for: 7 -> 8; matrix products, arithmetic and copies ran while one was open for 5% -> 7% of each run, Pallas kernels for 0% -> 0%
where the time goes in v1:
time: 193 us; the launch traced here: 192 us
  waiting for transfers between devices  134 us (69%)
  local copies, waits for them, and re-layouts  15.2 us (8%)
  between operations  15.2 us (8%)
  blocking collectives  14 us (7%)
  matrix products  8.4 us (4%)
  starting transfers between devices  5.5 us (3%)
    all_gather x1, waiting for transfers between devices, local(): lax.all_gather(dense_down, 'ep', axis=1, tiled=True)  39.9 us
    all_gather x1, waiting for transfers between devices, local(): lax.all_gather(dense_up, 'ep', axis=0, tiled=True)  39.5 us
    all_gather x1, waiting for transfers between devices, local(): lax.all_gather(dense_gate, 'ep', axis=0, tiled=True)  25.1 us
    ppermute x3, waiting for transfers between devices, swapped(): return lax.ppermute(block, axis, route)  15 us
    all_to_all x1, blocking collectives, local(): lax.all_to_all(split_rows, 'ep', split_axis=0, concat_axis=0, tiled=True)  14 us
    unnamed x23, local copies, waits for them, and re-layouts  12.1 us
    all_to_all x1, waiting for transfers between devices, local(): lax.all_to_all(jnp.stack(jnp.split(member_sums, lax.axis_size('ep'), axis...  8.2 us
    reduce_scatter x1, waiting for transfers between devices, local(): lax.psum_scatter(lax.dot_general(shard_rows, flat_hidden, (((0,), (1,)),...  4.29 us
  transfers between devices with their start and end apart: 9, of which 8 were waited for; matrix products, arithmetic and copies ran while one was open for 7% of the time, Pallas kernels for 0%

profile of v1, /device:TPU:0, one launch (start us, length us, event | category | flops | bytes accessed | tf_op | source)
XLA Modules:
  0.0 192.0 jit_solution(7165722620833087204)
XLA Ops:
  7.4 0.0 copy-start
  7.4 0.0 copy-start.5
  7.4 0.0 reduce-scatter.3.cloned.1.call-start
  7.4 0.7 copy-done.5
  8.1 1.6 gather_fusion
  9.8 0.1 fusion.10
  9.9 14.0 %all_to_all.10 = bf16[8,9,256]{2,1,0:T(8,128)(2,1)S(1)} all-to-all(bf16[8,9,256]{2,1,0:T(8,128)(2,1)S(1)} %fusion.10), channel_id=1, replica_groups=mesh['grp'=2,'ep'=8,'tp'=2] {'ep'}, dimensions={0} | all-to-all | bytes 73728 | tf_op jit(solution)/shard_map/all_to_all | solution.py:57
  23.9 0.5 collective-permute-start
  24.3 3.6 %collective-permute-done = bf16[8,9,1,256]{3,0,2,1:T(8,128)(2,1)S(1)} collective-permute-done((bf16[8,9,1,256]{3,0,2,1:T(8,128)(2,1)S(1)}, bf16[8,9,1,256]{3,0,2,1:T(8,128)(2,1)S(1)}, u32[]{:S(2)}, u32[]{:S(2)}) %collective-permute-start) | collective-permute-done | bytes 36896 | tf_op jit(solution)/shard_map/ppermute | solution.py:14
  27.9 0.3 collective-permute-start.1
  28.2 0.0 copy-start.2
  28.2 4.4 %collective-permute-done.1 = bf16[8,9,2,256]{3,0,2,1:T(8,128)(2,1)S(1)} collective-permute-done((bf16[8,9,2,256]{3,0,2,1:T(8,128)(2,1)S(1)}, bf16[8,9,2,256]{3,0,2,1:T(8,128)(2,1)S(1)}, u32[]{:S(2)}, u32[]{:S(2)}) %collective-permute-start.1) | collective-permute-done | bytes 73760 | tf_op jit(solution)/shard_map/ppermute | solution.py:14
  32.7 0.7 collective-permute-start.2
  33.4 6.9 %collective-permute-done.2 = bf16[8,9,4,256]{3,0,2,1:T(8,128)(2,1)S(1)} collective-permute-done((bf16[8,9,4,256]{3,0,2,1:T(8,128)(2,1)S(1)}, bf16[8,9,4,256]{3,0,2,1:T(8,128)(2,1)S(1)}, u32[]{:S(2)}, u32[]{:S(2)}) %collective-permute-start.2) | collective-permute-done | bytes 147488 | tf_op jit(solution)/shard_map/ppermute | solution.py:14
  40.4 0.1 copy.15
  40.4 0.0 copy-start.3
  40.4 0.1 copy.17
  40.5 0.0 copy-done.2
  40.5 0.3 fusion.33
  40.8 0.0 copy-done
  40.8 0.8 copy-done.3
  41.7 1.5 fusion
  43.1 0.0 reduce-scatter.3.cloned.1.call-update
  43.2 0.0 all-gather.4.cloned.1.call-start
  43.2 0.5 all-gather.4.cloned.1.call-update
  43.7 0.0 all-gather.6.cloned.1.call-start
  43.8 0.5 all-gather.6.cloned.1.call-update
  44.3 0.0 all-gather.8.cloned.1.call-start
  44.4 0.5 all-gather.8.cloned.1.call-update
  44.9 0.0 copy-start.1
  44.9 0.0 reduce-scatter.5.cloned.1.call-start
  45.0 4.3 %reduce-scatter.3.cloned.1.call-done = bf16[1024,72]{0,1:T(8,128)(2,1)} async-done(((bf16[2048,72]{0,1:T(8,128)(2,1)}), bf16[1024,72]{0,1:T(8,128)(2,1)}) %reduce-scatter.3.cloned.1.call-update) | async-done | bytes 147472 | tf_op jit(solution)/shard_map/reduce_scatter | solution.py:70
  49.3 1.4 fusion.24
  50.6 1.4 fusion.23
  52.0 1.4 fusion.22
  53.4 1.4 fusion.21
  54.9 1.4 fusion.20
  56.3 1.4 fusion.19
  57.7 1.4 fusion.18
  59.1 25.1 %all-gather.4.cloned.1.call-done = bf16[2048,256]{1,0:T(8,128)(2,1)} async-done(((bf16[256,256]{1,0:T(8,128)(2,1)}), bf16[2048,256]{1,0:T(8,128)(2,1)}) %all-gather.4.cloned.1.call-update) | async-done | bytes 1048592 | tf_op jit(solution)/shard_map/all_gather | solution.py:87
  84.2 0.0 copy-done.1
  84.2 1.5 fusion.34
  85.7 39.5 %all-gather.6.cloned.1.call-done = bf16[2048,256]{1,0:T(8,128)(2,1)} async-done(((bf16[256,256]{1,0:T(8,128)(2,1)}), bf16[2048,256]{1,0:T(8,128)(2,1)}) %all-gather.6.cloned.1.call-update) | async-done | bytes 1048592 | tf_op jit(solution)/shard_map/all_gather | solution.py:88
  125.2 39.9 %all-gather.8.cloned.1.call-done = bf16[256,2048]{1,0:T(8,128)(2,1)} async-done(((bf16[256,256]{1,0:T(8,128)(2,1)}), bf16[256,2048]{1,0:T(8,128)(2,1)}) %all-gather.8.cloned.1.call-update) | async-done | bytes 1048592 | tf_op jit(solution)/shard_map/all_gather | solution.py:95
  165.1 3.0 %convolution_convert_fusion.1 = bf16[64,2048]{1,0:T(8,128)(2,1)} fusion(bf16[256,2048]{1,0:T(8,128)(2,1)} %all-gather.8.cloned.1.call-done, bf16[64,2048]{1,0:T(8,128)(2,1)S(1)} %copy-done.1, bf16[2048,256]{1,0:T(8,128)(2,1)} %all-gather.6.cloned.1.call-done, f32[64,256]{1,0:T(8,128)S(1)} %fusion.34), kind=kOutput, calls=%fused_computation.2 | convolution fusion | flops 134447104 | bytes 2686976 | tf_op jit(solution)/shard_map/dot_general | solution.py:93
  168.2 0.0 reduce-scatter.5.cloned.1.call-update
  168.2 1.4 fusion.17
  169.6 0.0 copy-start.4
  169.6 3.9 %all-to-all-start.1 = ((bf16[8,1024,9]{1,2,0:T(8,128)(2,1)}), bf16[8,1024,9]{1,2,0:T(8,128)(2,1)S(1)}, u32[]{:S(2)}, u32[]{:S(2)}) async-start(bf16[8,1024,9]{1,2,0:T(8,128)(2,1)} %fusion.17), calls=%async_computation.2 | async-start | bytes 524288 | tf_op jit(solution)/shard_map/all_to_all | solution.py:79
  173.4 0.0 copy-done.4
  173.5 8.2 %all-to-all-done.1 = bf16[8,1024,9]{1,2,0:T(8,128)(2,1)S(1)} async-done(((bf16[8,1024,9]{1,2,0:T(8,128)(2,1)}), bf16[8,1024,9]{1,2,0:T(8,128)(2,1)S(1)}, u32[]{:S(2)}, u32[]{:S(2)}) %all-to-all-start.1) | async-done | bytes 147488 | tf_op jit(solution)/shard_map/all_to_all | solution.py:79
  181.7 0.0 reduce-scatter.5.cloned.1.call-done
  181.7 0.0 copy-start.6
  181.8 0.6 copy-done.6
  182.4 2.1 %fusion.1 = bf16[64,1024]{1,0:T(8,128)(2,1)} fusion(f32[1024,9]{0,1:T(8,128)S(1)} %convert_reduce_fusion, bf16[64,1024]{1,0:T(8,128)(2,1)} %reduce-scatter.5.cloned.1.call-done, f32[1024]{0:T(1024)S(1)} %add_divide_fusion, f32[9]{0:T(128)S(1)} %bitcast.74, s32[9]{0:T(128)S(1)} %bitcast.73), kind=kOutput, calls=%fused_computation.5 | convolution fusion | flops 7341184 | bytes 303176 | tf_op jit(solution)/shard_map/fek,ekt->tf/dot_general | solution.py:85
  (11 shorter events, 0.2 us)
Async XLA Ops:
  7.4 33.5 %copy-start = (bf16[256,2048]{1,0:T(8,128)(2,1)S(1)}, bf16[256,2048]{1,0:T(8,128)(2,1)}, u32[]{:S(2)}) copy-start(bf16[256,2048]{1,0:T(8,128)(2,1)} %param.15) | copy-start | bytes 3145732
  7.4 0.7 copy-start.5
  7.4 41.9 %reduce-scatter.3.cloned.1.call-start = ((), (), s32[]{:S(2)}) async-start(), calls=%async_computation.4 | async-start | bytes 442368 | tf_op jit(solution)/shard_map/reduce_scatter | solution.py:70
  23.9 4.0 %collective-permute-start = (bf16[8,9,1,256]{3,0,2,1:T(8,128)(2,1)S(1)}, bf16[8,9,1,256]{3,0,2,1:T(8,128)(2,1)S(1)}, u32[]{:S(2)}, u32[]{:S(2)}) collective-permute-start(bf16[8,9,1,256]{3,0,2,1:T(8,128)(2,1)S(1)} %bitcast.71), channel_id=1, source_target_pairs={{0,2},{2,0},{4,6},{6,4},{8,10},{10,8},{12,14},{14,12},{1,3},{3,1},... | collective-permute-start | bytes 110600 | tf_op jit(solution)/shard_map/ppermute | solution.py:14
  27.9 4.7 %collective-permute-start.1 = (bf16[8,9,2,256]{3,0,2,1:T(8,128)(2,1)S(1)}, bf16[8,9,2,256]{3,0,2,1:T(8,128)(2,1)S(1)}, u32[]{:S(2)}, u32[]{:S(2)}) collective-permute-start(bf16[8,9,2,256]{3,0,2,1:T(8,128)(2,1)S(1)} %maximum_select_fusion.2), channel_id=1, source_target_pairs={{0,4},{4,0},{2,6},{6,2},{8,12},{12,8},{10,14},{14,10},{1,5},{5,1},... | collective-permute-start | bytes 221192 | tf_op jit(solution)/shard_map/ppermute | solution.py:14
  28.2 12.3 %copy-start.2 = (bf16[2048,256]{1,0:T(8,128)(2,1)S(1)}, bf16[2048,256]{1,0:T(8,128)(2,1)}, u32[]{:S(2)}) copy-start(bf16[2048,256]{1,0:T(8,128)(2,1)} %param.13) | copy-start | bytes 3145732
  32.7 7.7 %collective-permute-start.2 = (bf16[8,9,4,256]{3,0,2,1:T(8,128)(2,1)S(1)}, bf16[8,9,4,256]{3,0,2,1:T(8,128)(2,1)S(1)}, u32[]{:S(2)}, u32[]{:S(2)}) collective-permute-start(bf16[8,9,4,256]{3,0,2,1:T(8,128)(2,1)S(1)} %maximum_select_fusion.1), channel_id=1, source_target_pairs={{0,8},{8,0},{2,10},{10,2},{4,12},{12,4},{6,14},{14,6},{1,9},{9,1},... | collective-permute-start | bytes 442376 | tf_op jit(solution)/shard_map/ppermute | solution.py:14
  40.4 1.2 copy-start.3
  43.2 41.0 %all-gather.4.cloned.1.call-start = ((), (), s32[]{:S(2)}) async-start(), calls=%async_computation.5 | async-start | bytes 1179648 | tf_op jit(solution)/shard_map/all_gather | solution.py:87
  43.7 81.5 %all-gather.6.cloned.1.call-start = ((), (), s32[]{:S(2)}) async-start(), calls=%async_computation.6 | async-start | bytes 1179648 | tf_op jit(solution)/shard_map/all_gather | solution.py:88
  44.3 120.8 %all-gather.8.cloned.1.call-start = ((), (), s32[]{:S(2)}) async-start(), calls=%async_computation.7 | async-start | bytes 1179648 | tf_op jit(solution)/shard_map/all_gather | solution.py:95
  44.9 39.3 %copy-start.1 = (bf16[64,2048]{1,0:T(8,128)(2,1)S(1)}, bf16[64,2048]{1,0:T(8,128)(2,1)}, u32[]{:S(2)}) copy-start(bf16[64,2048]{1,0:T(8,128)(2,1)} %param.10) | copy-start | bytes 786436
  44.9 136.8 %reduce-scatter.5.cloned.1.call-start = ((), (), s32[]{:S(2)}) async-start(), calls=%async_computation.8 | async-start | bytes 393216 | tf_op jit(solution)/shard_map/reduce_scatter | solution.py:98
  169.6 3.9 %copy-start.4 = (f32[1024]{0:T(1024)S(1)}, f32[1024]{0:T(1024)}, u32[]{:S(2)}) copy-start(f32[1024]{0:T(1024)} %param.19) | copy-start | bytes 12292
  169.6 12.1 %all-to-all-start.1 = ((bf16[8,1024,9]{1,2,0:T(8,128)(2,1)}), bf16[8,1024,9]{1,2,0:T(8,128)(2,1)S(1)}, u32[]{:S(2)}, u32[]{:S(2)}) async-start(bf16[8,1024,9]{1,2,0:T(8,128)(2,1)} %fusion.17), calls=%async_computation.2 | async-start | bytes 524288 | tf_op jit(solution)/shard_map/all_to_all | solution.py:79
  181.7 0.7 copy-start.6
Sparse Core Ops, SparseCore 0:
  43.3 5.9 reduce-scatter.2
  168.3 6.8 reduce-scatter.4
Sparse Core Ops, SparseCore 1:
  45.8 38.4 all-gather.3
  86.2 38.9 all-gather.5
  127.1 38.0 all-gather.7
